TPU v7x, 32 devices: a whole 2x2x4 slice. The times are simulated.
32 devices in a mesh: grp: 1, sp: 16 (over z, y, core), tp: 2 (over x).
Axes of the slice: x: 2, y: 2, z: 4, core: 2. Of those that a mesh axis runs over, the one named last changes fastest.
Arguments:
- residual: bfloat16 [8192, 2048], P(('grp', 'sp', 'tp')), may hold values from -6 to 6
- queries: bfloat16 [8192, 2048], P(('grp', 'sp'), 'tp'), may hold values from -200 to 200
- key_heads: bfloat16 [8192, 256], P(('grp', 'sp'), 'tp'), may hold values from -8 to 8
- value_heads: bfloat16 [8192, 256], P(('grp', 'sp'), 'tp'), may hold values from -6 to 6
- documents: int32 [8192], P(('grp', 'sp')), may hold values from 0 to 3, never falling along the last dimension, each value on 1 to 4096 neighbouring positions
- sink_logits: float32 [32], P('tp'), may hold values from 4 to 7
- out_weight: bfloat16 [2048, 2048], P('tp'), may hold values from -1 to 1
- norm_gain: bfloat16 [2048], replicated, may hold values from 0.099609375 to 1.8984375
- gate_weight: bfloat16 [2048, 5632], P('sp', 'tp'), may hold values from -0.125 to 0.125
- up_weight: bfloat16 [2048, 5632], P('sp', 'tp'), may hold values from -0.125 to 0.125
- down_weight: bfloat16 [2048, 5632], P('sp', 'tp'), may hold values from -0.078125 to 0.078125
Outputs:
- updated: bfloat16 [8192, 2048], P(('grp', 'sp', 'tp'))
Inputs may be any that keep to these rules, and one draw needn't show every extreme that they name: `documents`: document numbers never fall along the sequence.
All inputs are finite; a program needn't handle non-finite values.
Results may differ from a plain program's by a relative error of at most 0.012.
Values may be sent and summed in bfloat16 or wider, within the bound.
A program may use at most 128 MiB of HBM per device.

v0:
```python
import jax
import jax.numpy as jnp
from jax import lax
from jax.sharding import PartitionSpec as P

HD = 64
WINDOW = 128
epsilon = 1e-06
masked = -1e30


def padded(shard, sides, width):
    for axis, dim in sides:
        size, length = (lax.axis_size(axis), shard.shape[dim])
        up = [(i, (i + 1) % size) for i in range(size - 1)]
        down = [(j, i) for i, j in up]
        last = lax.slice_in_dim(shard, length - width, length, axis=dim)
        initial = lax.slice_in_dim(shard, 0, width, axis=dim)
        before = lax.ppermute(last, axis, up)
        after = lax.ppermute(initial, axis, down)
        shard = jnp.concatenate([before, shard, after], axis=dim)
    return shard


def on_device(
    residual,
    queries,
    key_heads,
    value_heads,
    documents,
    sink_logits,
    out_weight,
    norm_gain,
    gate_weight,
    up_weight,
    down_weight,
):
    tok_rows = queries.shape[0]
    kv_local = key_heads.shape[1] // HD
    q_local = queries.shape[1] // HD
    groups = q_local // kv_local
    own_docs = documents.astype(jnp.bfloat16)
    spread_keys, spread_values, spread_docs = (
        padded(key_heads, (("sp", 0),), WINDOW),
        padded(value_heads, (("sp", 0),), WINDOW),
        padded(own_docs, (("sp", 0),), WINDOW),
    )
    offset = lax.axis_index("sp") * tok_rows
    total_length = tok_rows * lax.axis_size("sp")
    query_pos = offset + jnp.arange(tok_rows, dtype=jnp.int32)
    key_pos = offset - WINDOW + jnp.arange(tok_rows + 2 * WINDOW, dtype=jnp.int32)
    allowed = (
        (jnp.abs(query_pos[:, None] - key_pos[None, :]) <= WINDOW)
        & (key_pos >= 0)[None, :]
        & (key_pos < total_length)[None, :]
        & (own_docs[:, None] == spread_docs[None, :])
    )
    query_block = queries.reshape(tok_rows, kv_local, groups, HD)
    key_block = spread_keys.reshape(-1, kv_local, HD)
    value_block = spread_values.reshape(-1, kv_local, HD)
    scores = jnp.einsum(
        "qkgd,jkd->kgqj", query_block, key_block, preferred_element_type=jnp.float32
    ) * HD ** (-0.5)
    scores = jnp.where(allowed[None, None], scores, masked)
    sink_table = sink_logits.reshape(kv_local, groups)[:, :, None]
    row_max = jnp.maximum(jnp.max(scores, axis=-1), sink_table)
    expo = jnp.exp(scores - row_max[..., None])
    total = jnp.sum(expo, axis=-1) + jnp.exp(sink_table - row_max)
    probs = (expo / total[..., None]).astype(jnp.bfloat16)
    mixed = jnp.einsum("kgqj,jkd->qkgd", probs, value_block, preferred_element_type=jnp.float32)
    attended = mixed.reshape(tok_rows, q_local * HD).astype(jnp.bfloat16)
    projected = lax.psum_scatter(
        jnp.dot(attended, out_weight, preferred_element_type=jnp.float32).astype(jnp.bfloat16),
        "tp",
        scatter_dimension=0,
        tiled=True,
    )
    middle = (
        residual.astype(jnp.float32) + lax.optimization_barrier(projected).astype(jnp.float32)
    ).astype(jnp.bfloat16)
    middle_wide = middle.astype(jnp.float32)
    scaled = middle_wide * lax.rsqrt(
        jnp.mean(middle_wide * middle_wide, axis=-1, keepdims=True) + epsilon
    )
    normed = (scaled * norm_gain.astype(jnp.float32)).astype(jnp.bfloat16)
    whole_gate, whole_up, whole_down = (
        lax.all_gather(gate_weight, "sp", axis=0, tiled=True),
        lax.all_gather(up_weight, "sp", axis=0, tiled=True),
        lax.all_gather(down_weight, "sp", axis=0, tiled=True),
    )
    row_piece = lax.all_gather(normed, "tp", axis=0, tiled=True)
    gate_value = jnp.dot(row_piece, whole_gate, preferred_element_type=jnp.float32)
    up_value = jnp.dot(row_piece, whole_up, preferred_element_type=jnp.float32)
    hidden = (jax.nn.silu(gate_value) * up_value).astype(jnp.bfloat16)
    mixer_out = lax.psum_scatter(
        lax.dot_general(
            hidden, whole_down, (((1,), (1,)), ((), ())), preferred_element_type=jnp.float32
        ).astype(jnp.bfloat16),
        "tp",
        scatter_dimension=0,
        tiled=True,
    )
    updated = middle.astype(jnp.float32) + 0.5 * lax.optimization_barrier(mixer_out).astype(
        jnp.float32
    )
    return updated.astype(jnp.bfloat16)


def solution(mesh):
    return jax.shard_map(
        on_device,
        mesh=mesh,
        in_specs=(
            P(("grp", "sp", "tp"), None),
            P(("grp", "sp"), "tp"),
            P(("grp", "sp"), "tp"),
            P(("grp", "sp"), "tp"),
            P(("grp", "sp")),
            P("tp"),
            P("tp", None),
            P(),
            P("sp", "tp"),
            P("sp", "tp"),
            P("sp", "tp"),
        ),
        out_specs=P(("grp", "sp", "tp"), None),
        check_vma=False,
    )
```

profile of v0, /device:TPU:0, one launch (start us, length us, event | category | flops | bytes accessed | tf_op | source)
XLA Modules:
  0.0 484.4 jit_solution(10772446977778538224)
XLA Ops:
  6.5 0.7 convert_element_type.50
  7.2 2.4 collective-permute-start.2
  9.6 1.3 collective-permute-start.3
  10.9 0.8 fusion.16
  11.7 5.1 %collective-permute-start.4 = (bf16[128,128]{1,0:T(8,128)(2,1)S(1)}, bf16[128,128]{1,0:T(8,128)(2,1)S(1)}, u32[]{:S(2)}, u32[]{:S(2)}) collective-permute-start(bf16[128,128]{1,0:T(8,128)(2,1)S(1)} %get-tuple-element.5), channel_id=1, source_target_pairs={{0,2},{2,4},{4,6},{6,8},{8,10},{10,12},{12,14},{14,16},{16,18},{18... | collective-permute-start | bytes 98312 | tf_op jit(solution)/shard_map/ppermute | solution.py:19
  16.9 1.3 collective-permute-start.5
  18.2 0.8 fusion.17
  18.9 4.3 collective-permute-start
  23.3 1.5 copy.18
  24.8 0.7 max.17
  25.5 0.0 collective-permute-done.2
  25.5 1.3 collective-permute-start.1
  26.8 1.0 fusion.9
  27.8 0.9 pad_maximum_fusion.1
  28.8 0.1 copy.17
  28.9 3.7 fusion.1
  32.7 0.1 broadcast_maximum_fusion
  32.7 5.2 %fusion = f32[2,8,512]{2,1,0:T(8,128)S(1)} fusion(f32[2,768,512,8]{2,1,3,0:T(8,128)S(1)} %get-tuple-element.12, f32[2,8,512]{2,1,0:T(8,128)S(1)} %broadcast_maximum_fusion, pred[512,768]{0,1:T(8,128)(4,1)S(1)} %fusion.9), kind=kLoop, calls=%fused_computation.3 | loop fusion | flops 25157632 | bytes 25624576 | tf_op jit(solution)/shard_map/reduce_sum | solution.py:68
  38.0 3.0 copy-done
  41.0 0.1 exponential_add_fusion
  41.2 0.1 copy.16
  41.3 0.0 copy-start.5
  41.3 12.0 %fusion.10 = bf16[2,64,8,512]{3,1,2,0:T(8,128)(2,1)S(1)} fusion(bf16[768,2,64,1]{0,2,3,1:T(8,128)(2,1)S(1)} %bitcast.37, f32[2,768,512,8]{2,1,3,0:T(8,128)} %copy-done, f32[2,8,512]{2,1,0:T(8,128)S(1)} %exponential_add_fusion, f32[2,8,512]{2,1,0:T(8,128)S(1)} %broadcast_maximum_fusion, pred[512,768]{0,1:T(8,128)(4,1)S(1)} %fusion.9), kind=kOutput, calls=%fused_computation.21 | convolution fusion | flops 837287936 | bytes 26869760 | tf_op jit(solution)/shard_map/kgqj,jkd->qkgd/dot_general | solution.py:70
  53.4 0.0 copy-start.4
  53.4 0.0 copy-start.1
  53.4 3.8 convolution_convert_fusion
  57.2 0.0 reduce-scatter.3.cloned.1.call-update
  57.2 0.0 all-gather.5.cloned.1.call-start
  57.3 37.5 %reduce-scatter.3.cloned.1.call-done = bf16[256,2048]{1,0:T(8,128)(2,1)} async-done(((bf16[512,2048]{1,0:T(8,128)(2,1)}), bf16[256,2048]{1,0:T(8,128)(2,1)}) %reduce-scatter.3.cloned.1.call-update) | async-done | bytes 1048592 | tf_op jit(solution)/shard_map/reduce_scatter | solution.py:72
  94.7 1.6 fusion.3
  96.4 2.6 fusion.5
  99.0 0.0 all-gather.5.cloned.1.call-update
  99.0 0.0 all-gather.7.cloned.1.call-start
  99.0 0.7 all-gather.7.cloned.1.call-update
  99.7 0.2 all-gather.11.cloned.1.call-start
  99.9 0.3 all-gather.11.cloned.1.call-update
  100.3 0.0 all-gather.9.cloned.1.call-start
  100.3 0.5 all-gather.9.cloned.1.call-update
  100.9 0.0 reduce-scatter.5.cloned.1.call-start
  100.9 31.3 %all-gather.5.cloned.1.call-done = bf16[512,2048]{1,0:T(8,128)(2,1)} async-done(((bf16[256,2048]{1,0:T(8,128)(2,1)}), bf16[512,2048]{1,0:T(8,128)(2,1)}) %all-gather.5.cloned.1.call-update) | async-done | bytes 2097168 | tf_op jit(solution)/shard_map/all_gather | solution.py:91
  132.2 96.3 %all-gather.7.cloned.1.call-done = bf16[2048,2816]{1,0:T(8,128)(2,1)} async-done(((bf16[128,2816]{1,0:T(8,128)(2,1)}), bf16[2048,2816]{1,0:T(8,128)(2,1)}) %all-gather.7.cloned.1.call-update) | async-done | bytes 11534352 | tf_op jit(solution)/shard_map/all_gather | solution.py:87
  228.5 12.5 %fusion.19 = f32[512,2816]{1,0:T(8,128)} fusion(bf16[512,2048]{1,0:T(8,128)(2,1)} %all-gather.5.cloned.1.call-done, bf16[2048,2816]{1,0:T(8,128)(2,1)} %all-gather.7.cloned.1.call-done), kind=kOutput, calls=%fused_computation.38 | convolution fusion | flops 5905580032 | bytes 19398656 | tf_op jit(solution)/shard_map/dot_general | solution.py:92
  241.0 81.9 %all-gather.11.cloned.1.call-done = bf16[2048,2816]{1,0:T(8,128)(2,1)} async-done(((bf16[128,2816]{1,0:T(8,128)(2,1)}), bf16[2048,2816]{1,0:T(8,128)(2,1)}) %all-gather.11.cloned.1.call-update) | async-done | bytes 11534352 | tf_op jit(solution)/shard_map/all_gather | solution.py:89
  322.9 94.4 %all-gather.9.cloned.1.call-done = bf16[2048,2816]{1,0:T(8,128)(2,1)} async-done(((bf16[128,2816]{1,0:T(8,128)(2,1)}), bf16[2048,2816]{1,0:T(8,128)(2,1)}) %all-gather.9.cloned.1.call-update) | async-done | bytes 11534352 | tf_op jit(solution)/shard_map/all_gather | solution.py:88
  417.3 27.3 %convolution_convert_fusion.1 = bf16[512,2048]{1,0:T(8,128)(2,1)} fusion(bf16[2048,2816]{1,0:T(8,128)(2,1)} %all-gather.11.cloned.1.call-done, f32[512,2816]{1,0:T(8,128)} %fusion.19, bf16[512,2048]{1,0:T(8,128)(2,1)} %all-gather.5.cloned.1.call-done, bf16[2048,2816]{1,0:T(8,128)(2,1)} %all-gather.9.cloned.1.call-done), kind=kOutput, calls=%fused_computation.11 | convolution fusion | flops 11820859392 | bytes 33030144 | tf_op jit(solution)/shard_map/dot_general | solution.py:96
  444.5 0.0 reduce-scatter.5.cloned.1.call-update
  444.6 30.3 %reduce-scatter.5.cloned.1.call-done = bf16[256,2048]{1,0:T(8,128)(2,1)} async-done(((bf16[512,2048]{1,0:T(8,128)(2,1)}), bf16[256,2048]{1,0:T(8,128)(2,1)}) %reduce-scatter.5.cloned.1.call-update) | async-done | bytes 1048592 | tf_op jit(solution)/shard_map/reduce_scatter | solution.py:95
  474.8 2.7 fusion.6
  (22 shorter events, 0.1 us)
Async XLA Ops:
  6.5 88.2 %reduce-scatter.3.cloned.1.call-start = ((), (), s32[]{:S(2)}) async-start(), calls=%async_computation.2 | async-start | bytes 3145728 | tf_op jit(solution)/shard_map/reduce_scatter | solution.py:72
  7.2 18.3 %collective-permute-start.2 = (bf16[128]{0:T(256)(128)(2,1)S(1)}, bf16[128]{0:T(256)(128)(2,1)S(1)}, u32[]{:S(2)}, u32[]{:S(2)}) collective-permute-start(bf16[128]{0:T(256)(128)(2,1)S(1)} %get-tuple-element.9), channel_id=1, source_target_pairs={{0,2},{2,4},{4,6},{6,8},{8,10},{10,12},{12,14},{14,16},{16,18},{18... | collective-permute-start | bytes 776 | tf_op jit(solution)/shard_map/ppermute | solution.py:19
  9.6 17.2 %collective-permute-start.3 = (bf16[128]{0:T(256)(128)(2,1)S(1)}, bf16[128]{0:T(256)(128)(2,1)S(1)}, u32[]{:S(2)}, u32[]{:S(2)}) collective-permute-start(bf16[128]{0:T(256)(128)(2,1)S(1)} %get-tuple-element.10), channel_id=1, source_target_pairs={{2,0},{4,2},{6,4},{8,6},{10,8},{12,10},{14,12},{16,14},{18,16},{20... | collective-permute-start | bytes 776 | tf_op jit(solution)/shard_map/ppermute | solution.py:20
  11.7 16.1 %collective-permute-start.4 = (bf16[128,128]{1,0:T(8,128)(2,1)S(1)}, bf16[128,128]{1,0:T(8,128)(2,1)S(1)}, u32[]{:S(2)}, u32[]{:S(2)}) collective-permute-start(bf16[128,128]{1,0:T(8,128)(2,1)S(1)} %get-tuple-element.5), channel_id=1, source_target_pairs={{0,2},{2,4},{4,6},{6,8},{8,10},{10,12},{12,14},{14,16},{16,18},{18... | collective-permute-start | bytes 98312 | tf_op jit(solution)/shard_map/ppermute | solution.py:19
  16.9 11.0 %collective-permute-start.5 = (bf16[128,128]{1,0:T(8,128)(2,1)S(1)}, bf16[128,128]{1,0:T(8,128)(2,1)S(1)}, u32[]{:S(2)}, u32[]{:S(2)}) collective-permute-start(bf16[128,128]{1,0:T(8,128)(2,1)S(1)} %get-tuple-element.6), channel_id=1, source_target_pairs={{2,0},{4,2},{6,4},{8,6},{10,8},{12,10},{14,12},{16,14},{18,16},{20... | collective-permute-start | bytes 98312 | tf_op jit(solution)/shard_map/ppermute | solution.py:20
  18.9 22.2 %collective-permute-start = (bf16[128,128]{1,0:T(8,128)(2,1)S(1)}, bf16[128,128]{1,0:T(8,128)(2,1)S(1)}, u32[]{:S(2)}, u32[]{:S(2)}) collective-permute-start(bf16[128,128]{1,0:T(8,128)(2,1)S(1)} %get-tuple-element.7), channel_id=1, source_target_pairs={{0,2},{2,4},{4,6},{6,8},{8,10},{10,12},{12,14},{14,16},{16,18},{18... | collective-permute-start | bytes 98312 | tf_op jit(solution)/shard_map/ppermute | solution.py:19
  25.5 15.6 %collective-permute-start.1 = (bf16[128,128]{1,0:T(8,128)(2,1)S(1)}, bf16[128,128]{1,0:T(8,128)(2,1)S(1)}, u32[]{:S(2)}, u32[]{:S(2)}) collective-permute-start(bf16[128,128]{1,0:T(8,128)(2,1)S(1)} %get-tuple-element.8), channel_id=1, source_target_pairs={{2,0},{4,2},{6,4},{8,6},{10,8},{12,10},{14,12},{16,14},{18,16},{20... | collective-permute-start | bytes 98312 | tf_op jit(solution)/shard_map/ppermute | solution.py:20
  32.7 8.4 %copy-start = (f32[2,768,512,8]{2,1,3,0:T(8,128)}, f32[2,768,512,8]{2,1,3,0:T(8,128)S(1)}, u32[]{:S(2)}) copy-start(f32[2,768,512,8]{2,1,3,0:T(8,128)S(1)} %get-tuple-element.12) | copy-start | bytes 75497472
  32.7 8.4 %copy-start.3 = (bf16[512,128]{1,0:T(8,128)(2,1)S(1)}, bf16[512,128]{1,0:T(8,128)(2,1)}, u32[]{:S(2)}) copy-start(bf16[512,128]{1,0:T(8,128)(2,1)} %param.14) | copy-start | bytes 393220
  41.3 12.0 %copy-start.5 = (bf16[1024,2048]{1,0:T(8,128)(2,1)S(1)}, bf16[1024,2048]{1,0:T(8,128)(2,1)}, u32[]{:S(2)}) copy-start(bf16[1024,2048]{1,0:T(8,128)(2,1)} %param.17) | copy-start | bytes 12582916
  53.4 3.9 copy-start.4
  53.4 41.3 %copy-start.1 = (bf16[256,2048]{1,0:T(8,128)(2,1)S(1)}, bf16[256,2048]{1,0:T(8,128)(2,1)}, u32[]{:S(2)}) copy-start(bf16[256,2048]{1,0:T(8,128)(2,1)} %param.11) | copy-start | bytes 3145732
  57.2 75.0 %all-gather.5.cloned.1.call-start = ((), (), s32[]{:S(2)}) async-start(), calls=%async_computation.3 | async-start | bytes 3145728 | tf_op jit(solution)/shard_map/all_gather | solution.py:91
  99.0 129.5 %all-gather.7.cloned.1.call-start = ((), (), s32[]{:S(2)}) async-start(), calls=%async_computation.4 | async-start | bytes 12255232 | tf_op jit(solution)/shard_map/all_gather | solution.py:87
  99.7 223.2 %all-gather.11.cloned.1.call-start = ((), (), s32[]{:S(2)}) async-start(), calls=%async_computation.6 | async-start | bytes 12255232 | tf_op jit(solution)/shard_map/all_gather | solution.py:89
  100.3 317.0 %all-gather.9.cloned.1.call-start = ((), (), s32[]{:S(2)}) async-start(), calls=%async_computation.5 | async-start | bytes 12255232 | tf_op jit(solution)/shard_map/all_gather | solution.py:88
  100.9 374.0 %reduce-scatter.5.cloned.1.call-start = ((), (), s32[]{:S(2)}) async-start(), calls=%async_computation.7 | async-start | bytes 3145728 | tf_op jit(solution)/shard_map/reduce_scatter | solution.py:95
  241.0 233.8 %copy-start.2 = (bf16[256,2048]{1,0:T(8,128)(2,1)S(1)}, bf16[256,2048]{1,0:T(8,128)(2,1)}, u32[]{:S(2)}) copy-start(bf16[256,2048]{1,0:T(8,128)(2,1)} %reduce-scatter.3.cloned.1.call-done) | copy-start | bytes 3145732
Sparse Core Ops, SparseCore 0:
  57.3 37.3 reduce-scatter.2
  99.1 33.0 all-gather.4
  134.5 93.9 all-gather.6
  230.7 92.2 all-gather.10
  325.0 92.2 all-gather.8
  444.7 30.1 reduce-scatter.4
where the time goes:
time: 485 us; the launch traced here: 484 us
  waiting for transfers between devices  373 us (77%)
  matrix products  59.3 us (12%)
  starting transfers between devices  16 us (3%)
  other arithmetic  15 us (3%)
  between operations  13.7 us (3%)
  local copies, waits for them, and re-layouts  7.17 us (1%)
    all_gather x1, waiting for transfers between devices, on_device(): lax.all_gather(gate_weight, 'sp', axis=0, tiled=True)  96.3 us
    all_gather x1, waiting for transfers between devices, on_device(): lax.all_gather(up_weight, 'sp', axis=0, tiled=True)  94.4 us
    all_gather x1, waiting for transfers between devices, on_device(): lax.all_gather(down_weight, 'sp', axis=0, tiled=True)  81.9 us
    reduce_scatter x1, waiting for transfers between devices, on_device(): lax.psum_scatter(jnp.dot(attended, out_weight, preferred_element_type=jnp...  37.5 us
    all_gather x1, waiting for transfers between devices, on_device(): row_piece = lax.all_gather(normed, 'tp', axis=0, tiled=True)  31.3 us
    reduce_scatter x1, waiting for transfers between devices, on_device(): lax.psum_scatter(lax.dot_general(hidden, whole_down, (((1,), (1,)), ((),...  30.3 us
    dot_general x1, matrix products, on_device(): lax.dot_general(hidden, whole_down, (((1,), (1,)), ((), ())), preferred_e...  27.3 us
    dot_general x1, matrix products, on_device(): jnp.dot(row_piece, whole_gate, preferred_element_type=jnp.float32)  12.5 us
  transfers between devices with their start and end apart: 12, of which 6 were waited for; matrix products, arithmetic and copies ran while one was open for 6% of the time, Pallas kernels for 0%

commit v1 on v0

--- a/solution.py
+++ b/solution.py
@@ -7,6 +7,13 @@
 WINDOW = 128
 epsilon = 1e-06
 masked = -1e30
+
+
+def meet_steps_all_now(a0):
+    spare = jnp.concatenate(
+        lax.all_to_all(jnp.stack([a0 for _ in range(lax.axis_size("sp"))], 0), "sp", 0, 0), axis=0
+    )
+    return spare
 
 
 def padded(shard, sides, width):
@@ -84,7 +91,7 @@
     )
     normed = (scaled * norm_gain.astype(jnp.float32)).astype(jnp.bfloat16)
     whole_gate, whole_up, whole_down = (
-        lax.all_gather(gate_weight, "sp", axis=0, tiled=True),
+        meet_steps_all_now(gate_weight),
         lax.all_gather(up_weight, "sp", axis=0, tiled=True),
         lax.all_gather(down_weight, "sp", axis=0, tiled=True),
     )

time: 485 us -> 577 us (1.19)
  waiting for transfers between devices: 373 us -> 454 us
    all_to_all x0 -> x1, waiting for transfers between devices: none -> 253 us  [meet_steps_all_now(): lax.all_to_all(jnp.stack([a0 for _ in range(lax.axis_size('sp'))], 0), 's...]
    all_gather x1 -> x0, waiting for transfers between devices: 96.3 us -> none  [on_device(): lax.all_gather(gate_weight, 'sp', axis=0, tiled=True)]
    all_gather x1, waiting for transfers between devices: 94.4 us -> 0.01 us  [on_device(): lax.all_gather(up_weight, 'sp', axis=0, tiled=True)]
    all_gather x1, waiting for transfers between devices: 81.9 us -> 105 us  [on_device(): lax.all_gather(down_weight, 'sp', axis=0, tiled=True)]
    all_gather x1, waiting for transfers between devices: 31.3 us -> 20.9 us  [on_device(): row_piece = lax.all_gather(normed, 'tp', axis=0, tiled=True)]
    reduce_scatter x1, waiting for transfers between devices: 30.3 us -> 36.3 us  [on_device(): lax.psum_scatter(lax.dot_general(hidden, whole_down, (((1,), (1,)), ((),...]
  transfers between devices with their start and end apart: 12 -> 12, of which waited for: 6 -> 5; matrix products, arithmetic and copies ran while one was open for 6% -> 6% of each run, Pallas kernels for 0% -> 0%
where the time goes in v1:
time: 577 us; the launch traced here: 576 us
  waiting for transfers between devices  454 us (79%)
  matrix products  59.7 us (10%)
  starting transfers between devices  21.6 us (4%)
  other arithmetic  15 us (3%)
  between operations  13.4 us (2%)
  local copies, waits for them, and re-layouts  12.4 us (2%)
    all_to_all x1, waiting for transfers between devices, meet_steps_all_now(): lax.all_to_all(jnp.stack([a0 for _ in range(lax.axis_size('sp'))], 0), 's...  253 us
    all_gather x1, waiting for transfers between devices, on_device(): lax.all_gather(down_weight, 'sp', axis=0, tiled=True)  105 us
    reduce_scatter x1, waiting for transfers between devices, on_device(): lax.psum_scatter(jnp.dot(attended, out_weight, preferred_element_type=jnp...  37.5 us
    reduce_scatter x1, waiting for transfers between devices, on_device(): lax.psum_scatter(lax.dot_general(hidden, whole_down, (((1,), (1,)), ((),...  36.3 us
    dot_general x1, matrix products, on_device(): lax.dot_general(hidden, whole_down, (((1,), (1,)), ((), ())), preferred_e...  27.2 us
    all_gather x1, waiting for transfers between devices, on_device(): row_piece = lax.all_gather(normed, 'tp', axis=0, tiled=True)  20.9 us
    dot_general x1, matrix products, on_device(): jnp.dot(row_piece, whole_gate, preferred_element_type=jnp.float32)  12.9 us
    dot_general x1, matrix products, on_device(): jnp.einsum('kgqj,jkd->qkgd', probs, value_block, preferred_element_type=j...  12 us
  transfers between devices with their start and end apart: 12, of which 5 were waited for; matrix products, arithmetic and copies ran while one was open for 6% of the time, Pallas kernels for 0%

profile of v1, /device:TPU:0, one launch (start us, length us, event | category | flops | bytes accessed | tf_op | source)
XLA Modules:
  0.0 576.1 jit_solution(10580042087553921983)
XLA Ops:
  6.5 0.7 convert_element_type.50
  7.2 2.4 collective-permute-start.2
  9.6 1.3 collective-permute-start.3
  10.9 0.8 fusion.16
  11.7 5.1 collective-permute-start.4
  16.9 1.3 collective-permute-start.5
  18.2 0.8 fusion.17
  18.9 4.3 collective-permute-start
  23.3 1.5 copy.18
  24.8 0.7 max.17
  25.5 0.0 collective-permute-done.2
  25.5 1.3 collective-permute-start.1
  26.8 0.0 collective-permute-done.3
  26.8 1.0 fusion.9
  27.8 0.9 pad_maximum_fusion.1
  28.8 0.1 copy.17
  28.9 3.7 fusion.1
  32.7 0.1 broadcast_maximum_fusion
  32.7 5.2 fusion
  38.0 3.0 copy-done
  41.0 0.1 exponential_add_fusion
  41.2 0.1 copy.16
  41.3 0.0 copy-start.6
  41.3 12.0 %fusion.10 = bf16[2,64,8,512]{3,1,2,0:T(8,128)(2,1)S(1)} fusion(bf16[768,2,64,1]{0,2,3,1:T(8,128)(2,1)S(1)} %bitcast.38, f32[2,768,512,8]{2,1,3,0:T(8,128)} %copy-done, f32[2,8,512]{2,1,0:T(8,128)S(1)} %exponential_add_fusion, f32[2,8,512]{2,1,0:T(8,128)S(1)} %broadcast_maximum_fusion, pred[512,768]{0,1:T(8,128)(4,1)S(1)} %fusion.9), kind=kOutput, calls=%fused_computation.21 | convolution fusion | flops 837287936 | bytes 26869760 | tf_op jit(solution)/shard_map/kgqj,jkd->qkgd/dot_general | solution.py:77
  53.4 0.0 copy-start.5
  53.4 0.0 copy-start.1
  53.4 3.8 convolution_convert_fusion
  57.2 0.0 reduce-scatter.3.cloned.1.call-update
  57.2 0.0 all-gather.4.cloned.1.call-start
  57.3 37.5 %reduce-scatter.3.cloned.1.call-done = bf16[256,2048]{1,0:T(8,128)(2,1)} async-done(((bf16[512,2048]{1,0:T(8,128)(2,1)}), bf16[256,2048]{1,0:T(8,128)(2,1)}) %reduce-scatter.3.cloned.1.call-update) | async-done | bytes 1048592 | tf_op jit(solution)/shard_map/reduce_scatter | solution.py:79
  94.7 1.6 fusion.3
  96.4 2.6 fusion.5
  99.0 0.0 all-gather.4.cloned.1.call-update
  99.0 0.2 all-gather.6.cloned.1.call-start
  99.2 0.5 all-gather.6.cloned.1.call-update
  99.7 5.3 stack.2
  105.0 5.7 all-to-all-start
  110.7 0.0 all-gather.8.cloned.1.call-start
  110.7 0.5 all-gather.8.cloned.1.call-update
  111.2 0.0 reduce-scatter.5.cloned.1.call-start
  111.3 20.9 %all-gather.4.cloned.1.call-done = bf16[512,2048]{1,0:T(8,128)(2,1)} async-done(((bf16[256,2048]{1,0:T(8,128)(2,1)}), bf16[512,2048]{1,0:T(8,128)(2,1)}) %all-gather.4.cloned.1.call-update) | async-done | bytes 2097168 | tf_op jit(solution)/shard_map/all_gather | solution.py:98
  132.2 253.4 %all-to-all-done = bf16[16,128,2816]{2,1,0:T(8,128)(2,1)} async-done(((bf16[16,128,2816]{2,1,0:T(8,128)(2,1)}), bf16[16,128,2816]{2,1,0:T(8,128)(2,1)}, u32[]{:S(2)}, u32[]{:S(2)}) %all-to-all-start) | async-done | bytes 11534368 | tf_op jit(solution)/shard_map/all_to_all | solution.py:14
  385.6 12.9 %fusion.19 = f32[512,2816]{1,0:T(8,128)} fusion(bf16[512,2048]{1,0:T(8,128)(2,1)} %all-gather.4.cloned.1.call-done, bf16[2048,2816]{1,0:T(8,128)(2,1)} %bitcast.10), kind=kOutput, calls=%fused_computation.38 | convolution fusion | flops 5905580032 | bytes 19398656 | tf_op jit(solution)/shard_map/dot_general | solution.py:99
  398.5 104.8 %all-gather.8.cloned.1.call-done = bf16[2048,2816]{1,0:T(8,128)(2,1)} async-done(((bf16[128,2816]{1,0:T(8,128)(2,1)}), bf16[2048,2816]{1,0:T(8,128)(2,1)}) %all-gather.8.cloned.1.call-update) | async-done | bytes 11534352 | tf_op jit(solution)/shard_map/all_gather | solution.py:96
  503.2 27.2 %convolution_convert_fusion.1 = bf16[512,2048]{1,0:T(8,128)(2,1)} fusion(bf16[2048,2816]{1,0:T(8,128)(2,1)} %all-gather.8.cloned.1.call-done, f32[512,2816]{1,0:T(8,128)} %fusion.19, bf16[512,2048]{1,0:T(8,128)(2,1)} %all-gather.4.cloned.1.call-done, bf16[2048,2816]{1,0:T(8,128)(2,1)} %all-gather.6.cloned.1.call-done), kind=kOutput, calls=%fused_computation.11 | convolution fusion | flops 11820859392 | bytes 33030144 | tf_op jit(solution)/shard_map/dot_general | solution.py:103
  530.5 0.0 reduce-scatter.5.cloned.1.call-update
  530.5 36.3 %reduce-scatter.5.cloned.1.call-done = bf16[256,2048]{1,0:T(8,128)(2,1)} async-done(((bf16[512,2048]{1,0:T(8,128)(2,1)}), bf16[256,2048]{1,0:T(8,128)(2,1)}) %reduce-scatter.5.cloned.1.call-update) | async-done | bytes 1048592 | tf_op jit(solution)/shard_map/reduce_scatter | solution.py:102
  566.8 2.7 fusion.6
  (24 shorter events, 0.1 us)
Async XLA Ops:
  6.5 88.2 %reduce-scatter.3.cloned.1.call-start = ((), (), s32[]{:S(2)}) async-start(), calls=%async_computation.3 | async-start | bytes 3145728 | tf_op jit(solution)/shard_map/reduce_scatter | solution.py:79
  7.2 18.3 %collective-permute-start.2 = (bf16[128]{0:T(256)(128)(2,1)S(1)}, bf16[128]{0:T(256)(128)(2,1)S(1)}, u32[]{:S(2)}, u32[]{:S(2)}) collective-permute-start(bf16[128]{0:T(256)(128)(2,1)S(1)} %get-tuple-element.9), channel_id=1, source_target_pairs={{0,2},{2,4},{4,6},{6,8},{8,10},{10,12},{12,14},{14,16},{16,18},{18... | collective-permute-start | bytes 776 | tf_op jit(solution)/shard_map/ppermute | solution.py:26
  9.6 17.2 %collective-permute-start.3 = (bf16[128]{0:T(256)(128)(2,1)S(1)}, bf16[128]{0:T(256)(128)(2,1)S(1)}, u32[]{:S(2)}, u32[]{:S(2)}) collective-permute-start(bf16[128]{0:T(256)(128)(2,1)S(1)} %get-tuple-element.10), channel_id=1, source_target_pairs={{2,0},{4,2},{6,4},{8,6},{10,8},{12,10},{14,12},{16,14},{18,16},{20... | collective-permute-start | bytes 776 | tf_op jit(solution)/shard_map/ppermute | solution.py:27
  11.7 16.1 %collective-permute-start.4 = (bf16[128,128]{1,0:T(8,128)(2,1)S(1)}, bf16[128,128]{1,0:T(8,128)(2,1)S(1)}, u32[]{:S(2)}, u32[]{:S(2)}) collective-permute-start(bf16[128,128]{1,0:T(8,128)(2,1)S(1)} %get-tuple-element.5), channel_id=1, source_target_pairs={{0,2},{2,4},{4,6},{6,8},{8,10},{10,12},{12,14},{14,16},{16,18},{18... | collective-permute-start | bytes 98312 | tf_op jit(solution)/shard_map/ppermute | solution.py:26
  16.9 11.0 %collective-permute-start.5 = (bf16[128,128]{1,0:T(8,128)(2,1)S(1)}, bf16[128,128]{1,0:T(8,128)(2,1)S(1)}, u32[]{:S(2)}, u32[]{:S(2)}) collective-permute-start(bf16[128,128]{1,0:T(8,128)(2,1)S(1)} %get-tuple-element.6), channel_id=1, source_target_pairs={{2,0},{4,2},{6,4},{8,6},{10,8},{12,10},{14,12},{16,14},{18,16},{20... | collective-permute-start | bytes 98312 | tf_op jit(solution)/shard_map/ppermute | solution.py:27
  18.9 22.2 %collective-permute-start = (bf16[128,128]{1,0:T(8,128)(2,1)S(1)}, bf16[128,128]{1,0:T(8,128)(2,1)S(1)}, u32[]{:S(2)}, u32[]{:S(2)}) collective-permute-start(bf16[128,128]{1,0:T(8,128)(2,1)S(1)} %get-tuple-element.7), channel_id=1, source_target_pairs={{0,2},{2,4},{4,6},{6,8},{8,10},{10,12},{12,14},{14,16},{16,18},{18... | collective-permute-start | bytes 98312 | tf_op jit(solution)/shard_map/ppermute | solution.py:26
  25.5 15.6 %collective-permute-start.1 = (bf16[128,128]{1,0:T(8,128)(2,1)S(1)}, bf16[128,128]{1,0:T(8,128)(2,1)S(1)}, u32[]{:S(2)}, u32[]{:S(2)}) collective-permute-start(bf16[128,128]{1,0:T(8,128)(2,1)S(1)} %get-tuple-element.8), channel_id=1, source_target_pairs={{2,0},{4,2},{6,4},{8,6},{10,8},{12,10},{14,12},{16,14},{18,16},{20... | collective-permute-start | bytes 98312 | tf_op jit(solution)/shard_map/ppermute | solution.py:27
  32.7 8.4 %copy-start = (f32[2,768,512,8]{2,1,3,0:T(8,128)}, f32[2,768,512,8]{2,1,3,0:T(8,128)S(1)}, u32[]{:S(2)}) copy-start(f32[2,768,512,8]{2,1,3,0:T(8,128)S(1)} %get-tuple-element.12) | copy-start | bytes 75497472
  32.7 8.4 %copy-start.4 = (bf16[512,128]{1,0:T(8,128)(2,1)S(1)}, bf16[512,128]{1,0:T(8,128)(2,1)}, u32[]{:S(2)}) copy-start(bf16[512,128]{1,0:T(8,128)(2,1)} %param.14) | copy-start | bytes 393220
  41.3 12.0 %copy-start.6 = (bf16[1024,2048]{1,0:T(8,128)(2,1)S(1)}, bf16[1024,2048]{1,0:T(8,128)(2,1)}, u32[]{:S(2)}) copy-start(bf16[1024,2048]{1,0:T(8,128)(2,1)} %param.17) | copy-start | bytes 12582916
  53.4 3.9 copy-start.5
  53.4 41.3 %copy-start.1 = (bf16[256,2048]{1,0:T(8,128)(2,1)S(1)}, bf16[256,2048]{1,0:T(8,128)(2,1)}, u32[]{:S(2)}) copy-start(bf16[256,2048]{1,0:T(8,128)(2,1)} %param.11) | copy-start | bytes 3145732
  57.2 42.6 %copy-start.3 = (bf16[128,2816]{1,0:T(8,128)(2,1)S(1)}, bf16[128,2816]{1,0:T(8,128)(2,1)}, u32[]{:S(2)}) copy-start(bf16[128,2816]{1,0:T(8,128)(2,1)} %param.19) | copy-start | bytes 2162692
  57.2 75.0 %all-gather.4.cloned.1.call-start = ((), (), s32[]{:S(2)}) async-start(), calls=%async_computation.4 | async-start | bytes 3145728 | tf_op jit(solution)/shard_map/all_gather | solution.py:98
  99.0 299.5 %all-gather.6.cloned.1.call-start = ((), (), s32[]{:S(2)}) async-start(), calls=%async_computation.5 | async-start | bytes 12255232 | tf_op jit(solution)/shard_map/all_gather | solution.py:95
  105.0 280.6 %all-to-all-start = ((bf16[16,128,2816]{2,1,0:T(8,128)(2,1)}), bf16[16,128,2816]{2,1,0:T(8,128)(2,1)}, u32[]{:S(2)}, u32[]{:S(2)}) async-start(bf16[16,128,2816]{2,1,0:T(8,128)(2,1)} %stack.2), calls=%async_computation.1 | async-start | bytes 23068672 | tf_op jit(solution)/shard_map/all_to_all | solution.py:14
  110.7 392.6 %all-gather.8.cloned.1.call-start = ((), (), s32[]{:S(2)}) async-start(), calls=%async_computation.6 | async-start | bytes 12255232 | tf_op jit(solution)/shard_map/all_gather | solution.py:96
  111.2 455.6 %reduce-scatter.5.cloned.1.call-start = ((), (), s32[]{:S(2)}) async-start(), calls=%async_computation.7 | async-start | bytes 3145728 | tf_op jit(solution)/shard_map/reduce_scatter | solution.py:102
  398.5 168.3 %copy-start.2 = (bf16[256,2048]{1,0:T(8,128)(2,1)S(1)}, bf16[256,2048]{1,0:T(8,128)(2,1)}, u32[]{:S(2)}) copy-start(bf16[256,2048]{1,0:T(8,128)(2,1)} %reduce-scatter.3.cloned.1.call-done) | copy-start | bytes 3145732
Sparse Core Ops, SparseCore 0:
  57.3 37.3 reduce-scatter.2
  99.1 33.0 all-gather.3
  134.5 230.4 all-gather.5
  367.1 136.0 all-gather.7
  530.6 36.1 reduce-scatter.4
